TPU v7x, 512 devices: a whole 4x8x8 slice. The times are simulated.
512 devices in a mesh: ep: 32 (over z, x), tp: 16 (over y, core).
Axes of the slice: x: 4, y: 8, z: 8, core: 2. Of those that a mesh axis runs over, the one named last changes fastest.
Arguments:
- queries: bfloat16 [16384, 2048], P('ep', 'tp'), may hold values from -5 to 5
- key_rows: bfloat16 [16384, 2048], P('ep', 'tp'), may hold values from -5 to 5
- values: bfloat16 [16384, 2048], P('ep', 'tp'), may hold values from -6 to 6
- forget_log: float32 [16384, 16], P(None, 'tp'), may hold values from -2051 to 0, as said below
- out_weight: bfloat16 [2048, 4096], P(None, 'tp'), may hold values from -1 to 1
- expert_input: bfloat16 [4096, 4096], P(('ep', 'tp')), may hold values from -6 to 6
- norm_gain: float32 [4096], replicated, may hold values from 0.1 to 1.9
- route_ids: int32 [4096, 2], P('ep'), may hold values from 0 to 31, all different within a row; in each aligned block of 128 rows (0 to 127, 128 to 255, ...) at most 16 rows name the same one
- route_weights: float32 [4096, 2], P('ep'), may hold values from 0.2 to 1
- gate_weight: bfloat16 [32, 4096, 2048], P('ep', None, 'tp'), may hold values from -0.09375 to 0.09375
- up_weight: bfloat16 [32, 4096, 2048], P('ep', None, 'tp'), may hold values from -0.09375 to 0.09375
- down_weight: bfloat16 [32, 2048, 4096], P('ep', None, 'tp'), may hold values from -0.125 to 0.125
Outputs:
- mixer_out: bfloat16 [16384, 4096], P('ep', 'tp')
- expert_out: bfloat16 [4096, 4096], P('ep', 'tp')
Inputs may be any that keep to these rules, and one draw needn't show every extreme that they name: forget_log[t, h] is the sum of the log forget gates of head h at positions 0 to t of the one sequence; it never rises along positions. `route_ids`: each row names 2 different experts. In each aligned block of 128 rows (the rows of one index of ep) no expert is named by more than 16 rows, and some block reaches 16.
All inputs are finite; a program needn't handle non-finite values.
Results may differ from a plain program's by a relative error of at most 0.0071.
Values may be sent and summed in bfloat16 or wider, within the bound.
A program may use at most 64 MiB of HBM per device.

v0:
```python
import jax
import jax.numpy as jnp
from jax import lax
from jax.sharding import Mesh
from jax.sharding import PartitionSpec as P

EP = ("ep_0", "ep_1")
EP_TP = ("ep_0", "ep_1", "tp")


EPSILON = 1e-05


def sent_together(arrays, axis, dim, along):
    widths = [a.shape[along] for a in arrays]
    both = jnp.concatenate(arrays, axis=along)
    filled = lax.all_gather(both, axis, axis=dim, tiled=True)
    return tuple(jnp.split(filled, [sum(widths[:k]) for k in range(1, len(widths))], axis=along))


def cut_along(value, dim, count):
    lengths = value.shape
    parts = value.reshape(*lengths[:dim], count, lengths[dim] // count, *lengths[dim + 1 :])
    return jnp.moveaxis(parts, dim, 0)


def in_order(parts, dim):
    lengths = list(parts.shape[1:])
    lengths[dim] *= parts.shape[0]
    return jnp.moveaxis(parts, 0, dim).reshape(lengths)


def exchange_in_order(parts, axes, sequence):
    inside = parts.shape[1:]
    filled = parts.reshape(*(lax.axis_size(a) for a in axes), *inside)
    for k in sequence:
        filled = lax.all_to_all(filled, axes[k], k, k, tiled=True)
    return filled.reshape(-1, *inside)


def stepwise_exchange(value, axes, sequence, split_dim, concat_dim):
    parts = cut_along(value, split_dim, lax.axis_size(axes))
    return in_order(exchange_in_order(parts, axes, sequence), concat_dim)


def slot_places(route_rows, experts, capacity):
    entries = route_rows.reshape(-1)
    matches = (entries[:, None] == jnp.arange(experts, dtype=jnp.int32)[None, :]).astype(jnp.int32)
    earlier = jnp.cumsum(matches, axis=0) - matches
    ranking = jnp.sum(earlier * matches, axis=1)
    return entries * capacity + ranking


def source_table(places, rows_count, chosen, total_slots):
    owners = jnp.arange(places.shape[0], dtype=jnp.int32) // chosen
    return jnp.full((total_slots,), rows_count, jnp.int32).at[places].set(owners)


def body(
    queries,
    key_rows,
    values,
    forget_log,
    out_weight,
    expert_input,
    norm_gain,
    route_ids,
    route_weights,
    gate_weight,
    up_weight,
    down_weight,
):
    row_count = queries.shape[0]
    heads_here = forget_log.shape[1]
    head_width = queries.shape[1] // heads_here
    own_start = lax.axis_index(EP) * row_count
    position_indices = own_start + jnp.arange(row_count, dtype=jnp.int32)
    query_heads = queries.reshape(row_count, heads_here, head_width)
    query_gate = lax.dynamic_slice_in_dim(forget_log, own_start, row_count, 0)
    score_scale = head_width ** (-0.5)

    def fold_shard(state_now, shard_item):
        first_row, key_shard, value_shard = shard_item

        def attend(state_in):
            row_max, row_total, weighted = state_in
            key_heads = key_shard.reshape(row_count, heads_here, head_width)
            value_heads = value_shard.reshape(row_count, heads_here, head_width)
            key_gate = lax.dynamic_slice_in_dim(forget_log, first_row, row_count, 0)
            scores = (
                jnp.einsum(
                    "qhd,khd->hqk", query_heads, key_heads, preferred_element_type=jnp.float32
                )
                * score_scale
            )
            scores = scores + query_gate.T[:, :, None] - key_gate.T[:, None, :]
            key_pos = first_row + jnp.arange(row_count, dtype=jnp.int32)
            scores = jnp.where(
                key_pos[None, None, :] <= position_indices[None, :, None], scores, -jnp.inf
            )
            newest = jnp.maximum(row_max, jnp.max(scores, axis=2))
            factor = jnp.exp(row_max - newest)
            weights_now = jnp.exp(scores - newest[:, :, None])
            row_total = row_total * factor + jnp.sum(weights_now, axis=2)
            weighted = weighted * factor[:, :, None] + jnp.einsum(
                "hqk,khd->hqd",
                weights_now.astype(jnp.bfloat16),
                value_heads,
                preferred_element_type=jnp.float32,
            )
            return (newest, row_total, weighted)

        return (
            lax.cond(first_row <= own_start, attend, lambda state_in: state_in, state_now),
            None,
        )

    initial = (
        jnp.full((heads_here, row_count), -jnp.inf, jnp.float32),
        jnp.zeros((heads_here, row_count), jnp.float32),
        jnp.zeros((heads_here, row_count, head_width), jnp.float32),
    )
    state_now = initial
    key_piece, value_piece = sent_together((key_rows, values), EP, 0, 1)
    shards = key_piece.shape[0] // row_count
    starts = row_count * jnp.arange(shards, dtype=jnp.int32)
    stacked = (
        starts,
        key_piece.reshape(shards, row_count, -1),
        value_piece.reshape(shards, row_count, -1),
    )
    state_now, _ = lax.scan(fold_shard, state_now, stacked)
    row_max, row_total, weighted = state_now
    attended = (
        (weighted / row_total[:, :, None])
        .transpose(1, 0, 2)
        .reshape(row_count, heads_here * head_width)
        .astype(jnp.bfloat16)
    )
    as_float = expert_input.astype(jnp.float32)
    center = jnp.mean(as_float, axis=1, keepdims=True)
    variance = jnp.mean(jnp.square(as_float - center), axis=1, keepdims=True)
    normed = ((as_float - center) * lax.rsqrt(variance + EPSILON) * norm_gain).astype(jnp.bfloat16)
    group_rows = lax.all_gather(normed, "tp", axis=0, tiled=True)
    block_rows = route_ids.shape[0]
    chosen = route_ids.shape[1]
    expert_local = gate_weight.shape[0]
    ep_count = lax.axis_size(EP)
    experts = expert_local * ep_count
    capacity = block_rows * chosen * 2 // experts
    places = slot_places(route_ids, experts, capacity)
    slot_table = source_table(places, block_rows, chosen, experts * capacity).reshape(
        ep_count, expert_local, capacity
    )
    outgoing = jnp.take(group_rows, slot_table, axis=0, mode="fill", fill_value=0)
    arrived = lax.all_to_all(outgoing, EP, split_axis=0, concat_axis=0, tiled=True)
    gate_part = jnp.einsum(
        "sxcd,xdf->sxcf", arrived, gate_weight, preferred_element_type=jnp.float32
    )
    up_part = jnp.einsum("sxcd,xdf->sxcf", arrived, up_weight, preferred_element_type=jnp.float32)
    hidden = (jax.nn.silu(gate_part) * up_part).astype(jnp.bfloat16)
    slots_all = ep_count * expert_local * capacity
    flat_hidden = hidden.reshape(slots_all, hidden.shape[3])
    out_width = out_weight.shape[1]
    mixer_sum = jnp.dot(
        lax.all_gather(attended, "tp", axis=1, tiled=True),
        out_weight,
        preferred_element_type=jnp.float32,
    )
    part_rows = lax.all_gather(flat_hidden, "tp", axis=1, tiled=True)
    shaped = part_rows.reshape(ep_count, expert_local, capacity, part_rows.shape[1])
    product = jnp.einsum("sxcf,xfd->sxcd", shaped, down_weight, preferred_element_type=jnp.float32)
    expert_sum = product.reshape(slots_all, out_width)
    leaving = expert_sum.astype(jnp.bfloat16).reshape(ep_count, expert_local, capacity, out_width)
    returned = stepwise_exchange(leaving, EP, (0, 1), 0, 0)
    picked = jnp.take(returned.reshape(experts * capacity, out_width), places, axis=0).astype(
        jnp.float32
    )
    combined = jnp.sum(
        (picked * route_weights.reshape(-1)[:, None]).reshape(block_rows, chosen, out_width), axis=1
    )
    return (mixer_sum.astype(jnp.bfloat16), combined.astype(jnp.bfloat16))


def solution(mesh):
    torus = Mesh(mesh.devices.reshape(8, 4, mesh.shape["tp"]), ("ep_0", "ep_1", "tp"))
    placed = (
        P(EP, "tp"),
        P(EP, "tp"),
        P(EP, "tp"),
        P(None, "tp"),
        P(None, "tp"),
        P(EP_TP, None),
        P(),
        P(EP, None),
        P(EP, None),
        P(EP, None, "tp"),
        P(EP, None, "tp"),
        P(EP, None, "tp"),
    )
    return jax.shard_map(
        body, mesh=torus, in_specs=placed, out_specs=(P(EP, "tp"), P(EP, "tp")), check_vma=False
    )
```

profile of v0, /device:TPU:1, one launch (start us, length us, event | category | flops | bytes accessed | tf_op | source)
XLA Modules:
  0.0 517.2 jit_solution(6071272296547223464)
XLA Ops:
  7.2 1.1 convert_reduce_fusion
  8.3 1.1 fusion.44
  9.4 1.6 fusion.46
  11.0 1.7 pad_maximum_fusion
  12.7 0.8 copy.30
  15.7 1.4 scatter_custom_fusion
  17.4 40.3 %all-gather.8.cloned.1.call-done = bf16[128,4096]{1,0:T(8,128)(2,1)} async-done(((bf16[8,4096]{1,0:T(8,128)(2,1)}), bf16[128,4096]{1,0:T(8,128)(2,1)}) %all-gather.8.cloned.1.call-update) | async-done | bytes 1048592 | tf_op jit(solution)/shard_map/all_gather | solution.py:144
  57.7 9.9 %gather_fusion = bf16[512,4096]{1,0:T(8,128)(2,1)} fusion(bf16[128,4096]{1,0:T(8,128)(2,1)} %all-gather.8.cloned.1.call-done, s32[1024]{0:T(1024)S(1)} %pad_clamp_fusion.1), kind=kCustom, calls=%fused_computation | custom fusion | bytes 8390656 | tf_op jit(solution)/shard_map/jit(_take)/gather | solution.py:155
  67.6 4.5 broadcast_select_fusion
  72.1 10.2 %all-to-all-start = ((bf16[32,1,16,4096]{3,2,1,0:T(8,128)(2,1)}), bf16[32,1,16,4096]{3,2,1,0:T(8,128)(2,1)}, u32[]{:S(2)}, u32[]{:S(2)}) async-start(bf16[32,1,16,4096]{3,2,1,0:T(8,128)(2,1)} %broadcast_select_fusion), calls=%async_computation | async-start | bytes 8388608 | tf_op jit(solution)/shard_map/all_to_all | solution.py:156
  82.4 0.8 constant_dynamic-slice_fusion.1
  83.1 124.5 %all-to-all-done = bf16[32,1,16,4096]{3,2,1,0:T(8,128)(2,1)} async-done(((bf16[32,1,16,4096]{3,2,1,0:T(8,128)(2,1)}), bf16[32,1,16,4096]{3,2,1,0:T(8,128)(2,1)}, u32[]{:S(2)}, u32[]{:S(2)}) %all-to-all-start) | async-done | bytes 4194336 | tf_op jit(solution)/shard_map/all_to_all | solution.py:156
  207.6 3.5 fusion.27
  211.1 4.1 fusion.36
  215.3 8.4 %all-gather.6.cloned.1.call-done = bf16[16384,256]{1,0:T(8,128)(2,1)} async-done(((bf16[512,256]{1,0:T(8,128)(2,1)}), bf16[16384,256]{1,0:T(8,128)(2,1)}) %all-gather.6.cloned.1.call-update) | async-done | bytes 8388624 | tf_op jit(solution)/shard_map/all_gather | solution.py:17
  223.7 5.7 %fusion.54 = (bf16[16384,128]{1,0:T(8,128)(2,1)}, bf16[16384,128]{1,0:T(8,128)(2,1)}) fusion(bf16[16384,256]{1,0:T(8,128)(2,1)} %all-gather.6.cloned.1.call-done), kind=kLoop, calls=%fused_computation.83 | loop fusion | bytes 16777216 | tf_op jit(solution)/shard_map/split | solution.py:18
  229.5 47.2 %while.16 = (s32[]{:T(128)}, f32[1,512]{1,0:T(1,128)S(1)}, f32[1,512]{1,0:T(1,128)S(1)}, f32[1,512,128]{2,1,0:T(8,128)S(1)}, s32[32]{0:T(128)S(1)}, /*index=5*/s...) while((s32[]{:T(128)}, f32[1,512]{1,0:T(1,128)S(1)}, ...), condition=%wide.region_5.6_spmd.clone.clone, body=%wide.region_0.5_spmd.clone.clone.sunk | while | flops 136972288 | bytes 4117845 | solution.py:132
  230.7 6.2 %conditional.4 = ((f32[1,512]{1,0:T(1,128)S(1)}, f32[1,512]{1,0:T(1,128)S(1)}, f32[1,512,128]{2,1,0:T(8,128)S(1)})) conditional(s32[]{:T(128)} %convert_element_type.103, (f32[1,512]{1,0:T(1,128)S(1)}, f32[1,512]{1,0:T(1,128)S(1)}, f32[1,512,128]{2,1,0:T(8,128)S(1)}) %tuple.49, (s32[]{:T(128)}, s32[]{:T(128)}, bf16[32,512,128]{2,1,0:T(8,128)(2,1)}, ...), branch_computations={%region_1.1_spmd, %region_2.4_spmd} | conditional | flops 136972288 | bytes 4115534 | solution.py:114
  232.7 0.8 constant_dynamic-slice_fusion
  234.1 1.3 fusion.53
  235.6 1.3 fusion.6
  276.7 0.8 divide_convert_fusion
  277.6 3.0 convolution_convert_fusion
  280.6 176.0 %all-to-all-start.1 = ((bf16[8,4,1,1,16,256]{5,4,1,3,2,0:T(8,128)(2,1)}), bf16[8,4,1,1,16,256]{5,4,1,3,2,0:T(8,128)(2,1)S(1)}, u32[]{:S(2)}, u32[]{:S(2)}) async-start(bf16[8,4,1,1,16,256]{5,4,1,3,2,0:T(8,128)(2,1)} %bitcast.42), calls=%async_computation.1 | async-start | bytes 524288 | tf_op jit(solution)/shard_map/all_to_all | solution.py:37
  456.7 10.6 %all-to-all-done.1 = bf16[8,4,1,1,16,256]{5,4,1,3,2,0:T(8,128)(2,1)S(1)} async-done(((bf16[8,4,1,1,16,256]{5,4,1,3,2,0:T(8,128)(2,1)}), bf16[8,4,1,1,16,256]{5,4,1,3,2,0:T(8,128)(2,1)S(1)}, u32[]{:S(2)}, u32[]{:S(2)}) %all-to-all-start.1) | async-done | bytes 262176 | tf_op jit(solution)/shard_map/all_to_all | solution.py:37
  467.3 0.7 copy.38
  468.0 21.4 %all-to-all-start.2 = ((bf16[8,4,1,1,16,256]{5,4,0,3,2,1:T(8,128)(2,1)}), bf16[8,4,1,1,16,256]{5,4,0,3,2,1:T(8,128)(2,1)S(1)}, u32[]{:S(2)}, u32[]{:S(2)}) async-start(bf16[8,4,1,1,16,256]{5,4,0,3,2,1:T(8,128)(2,1)} %copy.38), calls=%async_computation.2 | async-start | bytes 524288 | tf_op jit(solution)/shard_map/all_to_all | solution.py:37
  489.7 5.3 %all-to-all-done.2 = bf16[8,4,1,1,16,256]{5,4,0,3,2,1:T(8,128)(2,1)S(1)} async-done(((bf16[8,4,1,1,16,256]{5,4,0,3,2,1:T(8,128)(2,1)}), bf16[8,4,1,1,16,256]{5,4,0,3,2,1:T(8,128)(2,1)S(1)}, u32[]{:S(2)}, u32[]{:S(2)}) %all-to-all-start.2) | async-done | bytes 262176 | tf_op jit(solution)/shard_map/all_to_all | solution.py:37
  495.0 1.2 gather_fusion.1
  496.2 1.8 multiply_reduce_fusion
  498.0 9.6 %all-gather.12.cloned.1.call-done = bf16[1,512,2048]{2,1,0:T(8,128)(2,1)} async-done(((bf16[1,512,128]{2,1,0:T(8,128)(2,1)}), bf16[1,512,2048]{2,1,0:T(8,128)(2,1)}) %all-gather.12.cloned.1.call-update) | async-done | bytes 2097168 | tf_op jit(solution)/shard_map/all_gather | solution.py:166
  507.7 3.0 fusion.24
  (156 shorter events, 23.4 us)
Async XLA Ops:
  7.2 270.4 %copy-start = (bf16[1,2048,256]{2,1,0:T(8,128)(2,1)S(1)}, bf16[1,2048,256]{2,1,0:T(8,128)(2,1)}, u32[]{:S(2)}) copy-start(bf16[1,2048,256]{2,1,0:T(8,128)(2,1)} %param.27) | copy-start | bytes 3145732
  7.2 50.5 %all-gather.8.cloned.1.call-start = ((), (), s32[]{:S(2)}) async-start(), calls=%async_computation.4 | async-start | bytes 1114112 | tf_op jit(solution)/shard_map/all_gather | solution.py:144
  10.9 212.8 %all-gather.6.cloned.1.call-start = ((), (), s32[]{:S(2)}) async-start(), calls=%async_computation.3 | async-start | bytes 8650752 | tf_op jit(solution)/shard_map/all_gather | solution.py:17
  72.1 135.5 %copy-start.1 = (bf16[1,4096,128]{2,1,0:T(8,128)(2,1)S(1)}, bf16[1,4096,128]{2,1,0:T(8,128)(2,1)}, u32[]{:S(2)}) copy-start(bf16[1,4096,128]{2,1,0:T(8,128)(2,1)} %param.25) | copy-start | bytes 3145732
  72.1 135.5 %all-to-all-start = ((bf16[32,1,16,4096]{3,2,1,0:T(8,128)(2,1)}), bf16[32,1,16,4096]{3,2,1,0:T(8,128)(2,1)}, u32[]{:S(2)}, u32[]{:S(2)}) async-start(bf16[32,1,16,4096]{3,2,1,0:T(8,128)(2,1)} %broadcast_select_fusion), calls=%async_computation | async-start | bytes 8388608 | tf_op jit(solution)/shard_map/all_to_all | solution.py:156
  82.3 128.8 %copy-start.4 = (bf16[1,4096,128]{2,1,0:T(8,128)(2,1)S(1)}, bf16[1,4096,128]{2,1,0:T(8,128)(2,1)}, u32[]{:S(2)}) copy-start(bf16[1,4096,128]{2,1,0:T(8,128)(2,1)} %param.26) | copy-start | bytes 3145732
  82.3 195.3 %all-gather.10.cloned.1.call-start = ((), (), s32[]{:S(2)}) async-start(), calls=%async_computation.5 | async-start | bytes 2228224 | tf_op jit(solution)/shard_map/all_gather | solution.py:170
  215.2 14.2 %copy-start.6 = (bf16[512,128]{1,0:T(8,128)(2,1)S(1)}, bf16[512,128]{1,0:T(8,128)(2,1)}, u32[]{:S(2)}) copy-start(bf16[512,128]{1,0:T(8,128)(2,1)} %param.16) | copy-start | bytes 393220
  215.3 292.4 %all-gather.12.cloned.1.call-start = ((), (), s32[]{:S(2)}) async-start(), calls=%async_computation.6 | async-start | bytes 2228224 | tf_op jit(solution)/shard_map/all_gather | solution.py:166
  276.7 212.7 %copy-start.2 = (s32[128,2]{0,1:T(2,128)S(1)}, s32[128,2]{0,1:T(2,128)}, u32[]{:S(2)}) copy-start(s32[128,2]{0,1:T(2,128)} %param.23) | copy-start | bytes 3076
  276.7 212.9 %copy-start.3 = (f32[128,2]{0,1:T(2,128)S(1)}, f32[128,2]{0,1:T(2,128)}, u32[]{:S(2)}) copy-start(f32[128,2]{0,1:T(2,128)} %param.24) | copy-start | bytes 3076
  276.7 231.0 %copy-start.5 = (bf16[2048,256]{1,0:T(8,128)(2,1)S(1)}, bf16[2048,256]{1,0:T(8,128)(2,1)}, u32[]{:S(2)}) copy-start(bf16[2048,256]{1,0:T(8,128)(2,1)} %param.20) | copy-start | bytes 3145732
  280.6 186.7 %all-to-all-start.1 = ((bf16[8,4,1,1,16,256]{5,4,1,3,2,0:T(8,128)(2,1)}), bf16[8,4,1,1,16,256]{5,4,1,3,2,0:T(8,128)(2,1)S(1)}, u32[]{:S(2)}, u32[]{:S(2)}) async-start(bf16[8,4,1,1,16,256]{5,4,1,3,2,0:T(8,128)(2,1)} %bitcast.42), calls=%async_computation.1 | async-start | bytes 524288 | tf_op jit(solution)/shard_map/all_to_all | solution.py:37
  468.0 27.0 %all-to-all-start.2 = ((bf16[8,4,1,1,16,256]{5,4,0,3,2,1:T(8,128)(2,1)}), bf16[8,4,1,1,16,256]{5,4,0,3,2,1:T(8,128)(2,1)S(1)}, u32[]{:S(2)}, u32[]{:S(2)}) async-start(bf16[8,4,1,1,16,256]{5,4,0,3,2,1:T(8,128)(2,1)} %copy.38), calls=%async_computation.2 | async-start | bytes 524288 | tf_op jit(solution)/shard_map/all_to_all | solution.py:37
Sparse Core Ops, SparseCore 0:
  11.1 46.5 all-gather.7
  61.4 162.2 all-gather.5
  225.8 40.3 all-gather.9
  277.7 229.9 all-gather.11
where the time goes:
time: 521 us; the launch traced here: 517 us
  starting transfers between devices  208 us (40%)
  waiting for transfers between devices  199 us (38%)
  local copies, waits for them, and re-layouts  41.6 us (8%)
  loops' own time  24.1 us (5%)
  matrix products  16.2 us (3%)
  other arithmetic  14.8 us (3%)
  between operations  14 us (3%)
    all_to_all x2, starting transfers between devices, exchange_in_order(): filled = lax.all_to_all(filled, axes[k], k, k, tiled=True)  197 us
    all_to_all x1, waiting for transfers between devices, body(): lax.all_to_all(outgoing, EP, split_axis=0, concat_axis=0, tiled=True)  124 us
    all_gather x1, waiting for transfers between devices, body(): group_rows = lax.all_gather(normed, 'tp', axis=0, tiled=True)  40.3 us
    another operation x1, loops' own time, body(): state_now, _ = lax.scan(fold_shard, state_now, stacked)  21.7 us
    dynamic_slice x32, local copies, waits for them, and re-layouts, body(): state_now, _ = lax.scan(fold_shard, state_now, stacked)  18.8 us
    all_to_all x2, waiting for transfers between devices, exchange_in_order(): filled = lax.all_to_all(filled, axes[k], k, k, tiled=True)  15.9 us
  transfers between devices with their start and end apart: 7, of which 6 were waited for; matrix products, arithmetic and copies ran while one was open for 13% of the time, Pallas kernels for 0%

commit v1 on v0

v1 whole, which is shorter than its diff:
```python
import math

import jax
import jax.numpy as jnp
from jax import lax
from jax.experimental import pallas as pl
from jax.experimental.pallas import tpu as pltpu
from jax.sharding import PartitionSpec as P

MESH = pl.DeviceIdType.MESH
EPSILON = 1e-05
LOG2E = math.log2(math.e)
LOW = -1e30
NT = (((1,), (1,)), ((), ()))
NN = (((1,), (0,)), ((), ()))
TN = (((0,), (0,)), ((), ()))
F32 = jnp.float32
BF16 = jnp.bfloat16

NX, NZ, NE = 4, 8, 32
NY, NTP = 8, 16
ROWS, HD, D = 512, 128, 4096
CAP, TOK, WIDE = 16, 128, 256
SLOTS = NE * CAP
GROUP = NX * ROWS


def dot(a, b, dims):
    return lax.dot_general(a, b, dims, preferred_element_type=F32)


def kernel(
    q_ref, k_ref, v_ref, fl_ref, xin_ref, gain_ref, ids_ref, rw_ref,
    gate_hbm, up_hbm, down_hbm, out_hbm,
    mix_ref, exp_ref,
    k4, vt4, q8, bias, po_out, ps_out, po_in, ps_in, m_s, l_s, acc_s, num_s, den_s, top_s,
    xs, tok, disp, gath, accg, hb, accd, res, ret, ab, accm,
    wgu, wd, wo,
    w_sem, kv_send, kv_recv, q_send, q_recv, tok_send, tok_recv, d_send, d_recv,
    po_send, po_recv, ps_send, ps_recv,
    g_send, g_recv, h_send, h_recv, a_send, a_recv, b_send, b_recv,
):
    e = lax.axis_index("ep")
    t = lax.axis_index("tp")
    z, x = lax.div(e, NX), lax.rem(e, NX)
    y, c = lax.div(t, 2), lax.rem(t, 2)

    def remote(src, dst, ssem, rsem, ep, tp):
        return pltpu.make_async_remote_copy(
            src_ref=src, dst_ref=dst, send_sem=ssem, recv_sem=rsem,
            device_id=(ep, tp), device_id_type=MESH,
        )

    def each(low, high, fn):
        def step(i, carry):
            fn(i)
            return carry
        lax.fori_loop(low, high, step, 0)

    weights = (
        pltpu.make_async_copy(gate_hbm, wgu.at[:, pl.ds(0, 128)], w_sem.at[0]),
        pltpu.make_async_copy(up_hbm, wgu.at[:, pl.ds(128, 128)], w_sem.at[1]),
        pltpu.make_async_copy(down_hbm, wd, w_sem.at[2]),
        pltpu.make_async_copy(out_hbm, wo, w_sem.at[3]),
    )
    for copy in weights:
        copy.start()

    barrier = pltpu.get_barrier_semaphore()

    def greet_ep(i):
        pl.semaphore_signal(
            barrier, inc=1, device_id=(lax.rem(e + i, NE), t), device_id_type=MESH
        )

    def greet_tp(i):
        pl.semaphore_signal(
            barrier, inc=1, device_id=(e, lax.rem(t + i, NTP)), device_id_type=MESH
        )

    each(1, NE, greet_ep)
    each(1, NTP, greet_tp)

    rows = xin_ref[...].astype(F32)
    center = jnp.mean(rows, axis=1, keepdims=True)
    spread = rows - center
    variance = jnp.mean(spread * spread, axis=1, keepdims=True)
    normed = (spread * lax.rsqrt(variance + EPSILON) * gain_ref[...]).astype(BF16).astype(F32)
    for i in range(NTP):
        xs[i] = normed[:, WIDE * i : WIDE * (i + 1)]
    tok[t] = xs[t]
    k4[x] = k_ref[...]
    vt4[x] = v_ref[...].astype(F32).T.astype(BF16)
    q8[z] = q_ref[...]

    ids = ids_ref[...]
    experts = lax.broadcasted_iota(jnp.int32, (NE, TOK), 0)
    match = [(experts == ids[i : i + 1, :]).astype(F32) for i in range(2)]
    before = (
        lax.broadcasted_iota(jnp.int32, (TOK, TOK), 0)
        < lax.broadcasted_iota(jnp.int32, (TOK, TOK), 1)
    ).astype(F32).astype(BF16)
    earlier = dot((match[0] + match[1]).astype(BF16), before, NN)
    slot_rows = lax.broadcasted_iota(jnp.int32, (SLOTS, TOK), 0)
    places = [
        ids[i : i + 1, :] * CAP
        + jnp.sum(earlier * match[i], axis=0, keepdims=True).astype(jnp.int32)
        for i in range(2)
    ]

    def picks(i):
        return (slot_rows == places[i]).astype(F32)

    pl.semaphore_wait(barrier, NE + NTP - 2)

    def tok_copy(i, peer):
        return remote(xs.at[peer], tok.at[t], tok_send.at[i], tok_recv.at[t], e, peer)

    each(1, NTP, lambda i: tok_copy(i, lax.rem(t + i, NTP)).start())

    def kv_copies(i):
        peer = z * NX + lax.rem(x + i, NX)
        return (
            remote(k4.at[x], k4.at[x], kv_send.at[i], kv_recv.at[x], peer, t),
            remote(vt4.at[x], vt4.at[x], kv_send.at[NX + i], kv_recv.at[NX + x], peer, t),
        )

    for i in range(1, NX):
        for copy in kv_copies(i):
            copy.start()

    def tok_arrive(i):
        src = lax.rem(t + i, NTP)
        remote(xs.at[src], tok.at[src], tok_send.at[i], tok_recv.at[src], e, src).wait_recv()

    each(1, NTP, tok_arrive)
    routed = (picks(0) + picks(1)).astype(BF16)
    tokens = tok[...].reshape(TOK, WIDE).astype(BF16)
    disp[...] = dot(routed, tokens, NN).astype(BF16).reshape(NE, CAP, WIDE)
    gath[t, e] = disp[e]

    def d_copy(i):
        peer = lax.rem(e + i, NE)
        return remote(disp.at[peer], gath.at[t, e], d_send.at[i], d_recv.at[e], peer, t)

    each(1, NE, lambda i: d_copy(i).start())

    def q_copy(zz):
        return remote(q8.at[z], q8.at[z], q_send.at[zz], q_recv.at[z], zz * NX + x, t)

    each(0, z, lambda i: q_copy(z - 1 - i).start())

    key_row = fl_ref[:, pl.ds(pl.multiple_of(z * GROUP, GROUP), GROUP)]
    base = key_row[:, 0:1]
    bias_row = (base - key_row) * LOG2E
    for i in range(GROUP // 128):
        piece = bias_row[:, 128 * i : 128 * (i + 1)]
        bias[pl.ds(128 * i, 128), :] = jnp.broadcast_to(piece, (128, 128)).T

    for i in range(1, NX):
        src = lax.rem(x + i, NX)
        remote(k4.at[src], k4.at[src], kv_send.at[i], kv_recv.at[src], e, t).wait_recv()
        remote(vt4.at[src], vt4.at[src], kv_send.at[i], kv_recv.at[NX + src], e, t).wait_recv()

    unit_scale = LOG2E * HD ** (-0.5)

    def logits(b, queries):
        shift = bias[pl.ds(ROWS * b, ROWS), :]
        shift = jnp.concatenate([shift, shift], axis=1)
        return dot(k4[b], queries, NT) * unit_scale + shift

    def query_shift(k, h):
        start = pl.multiple_of((x + NX * k) * ROWS + WIDE * h, WIDE)
        return (fl_ref[:, pl.ds(start, WIDE)] - base) * LOG2E

    def fold(state, b, scores):
        top, total, acc = state
        newest = jnp.maximum(top, jnp.max(scores, axis=0, keepdims=True))
        factor = jnp.exp2(top - newest)
        weights_now = jnp.exp2(scores - newest)
        total = total * factor + jnp.sum(weights_now, axis=0, keepdims=True)
        acc = acc * factor + dot(vt4[b], weights_now.astype(BF16), NN)
        return newest, total, acc

    def fresh():
        return (
            jnp.full((1, WIDE), LOW, F32),
            jnp.zeros((1, WIDE), F32),
            jnp.zeros((HD, WIDE), F32),
        )

    for h in range(2):
        lanes = pl.ds(WIDE * h, WIDE)
        m_s[...], l_s[...], acc_s[...] = fresh()
        ahead = lax.broadcasted_iota(jnp.int32, (ROWS, WIDE), 0) - lax.broadcasted_iota(
            jnp.int32, (ROWS, WIDE), 1
        )

        def chunk(b):
            scores = logits(b, q8[z, pl.ds(WIDE * h, WIDE), :])
            scores = jnp.where(ahead <= WIDE * h + ROWS * (x - b), scores, LOW)
            m_s[...], l_s[...], acc_s[...] = fold((m_s[...], l_s[...], acc_s[...]), b, scores)

        each(0, x + 1, chunk)
        num_s[:, lanes] = acc_s[...] / l_s[...]
        top_s[:, lanes] = m_s[...] + jnp.log2(l_s[...]) + query_shift(z, h)
        den_s[:, lanes] = jnp.ones((1, WIDE), F32)

    def po_copies(k):
        return (
            remote(po_out.at[k], po_in.at[z], po_send.at[k], po_recv.at[z], k * NX + x, t),
            remote(ps_out.at[k], ps_in.at[z], ps_send.at[k], ps_recv.at[z], k * NX + x, t),
        )

    def unit(k):
        remote(q8.at[k], q8.at[k], q_send.at[k], q_recv.at[k], e, t).wait_recv()
        for h in range(2):
            queries = q8[k, pl.ds(WIDE * h, WIDE), :]
            state = fresh()
            for b in range(NX):
                state = fold(state, b, logits(b, queries))
            top, total, acc = state
            po_out[k, :, pl.ds(WIDE * h, WIDE)] = (acc / total).astype(BF16)
            ps_out[k, :, pl.ds(WIDE * h, WIDE)] = top + jnp.log2(total) + query_shift(k, h)
        for copy in po_copies(k):
            copy.start()

    def units(first, last):
        each(jnp.minimum(z + first, NZ), jnp.minimum(z + last, NZ), unit)

    def ring(buf, ssem, rsem, half, consume, between):
        right, left = 2 * lax.rem(y + 1, NY) + c, 2 * lax.rem(y + NY - 1, NY) + c
        other = 1 - 2 * c
        started = []

        def copy(src, i, r, tp):
            return remote(src, src, ssem.at[i], rsem.at[r], e, tp)

        def send(src, r, tp):
            one = copy(src, len(started), r, tp)
            one.start()
            started.append(one)

        def arrive(src, r):
            copy(src, 0, r, right).wait_recv()

        def slot_of(step):
            return 2 * lax.rem(y + step + NY, NY) + c

        near = pl.ds(0, half)
        far = pl.ds(half, half)
        send(buf.at[t], t, right)
        send(buf.at[t], t, left)
        send(buf.at[t], t, t + other)
        consume(t)
        earlier_slots = [t]
        for s in range(1, 4):
            a, b = slot_of(-s), slot_of(s)
            arrive(buf.at[a], a)
            send(buf.at[a] if s < 3 else buf.at[a, near], a if s < 3 else NTP, right)
            send(buf.at[a], a, t + other)
            arrive(buf.at[b], b)
            send(buf.at[b] if s < 3 else buf.at[b, far], b if s < 3 else NTP + 1, left)
            send(buf.at[b], b, t + other)
            between(s)
            consume(a)
            consume(b)
            for slot in earlier_slots:
                arrive(buf.at[slot + other], slot + other)
                consume(slot + other)
            earlier_slots = [a, b]
        a = slot_of(4)
        arrive(buf.at[a, near], NTP)
        arrive(buf.at[a, far], NTP + 1)
        send(buf.at[a], a, t + other)
        between(4)
        consume(a)
        for slot in earlier_slots + [a]:
            arrive(buf.at[slot + other], slot + other)
            consume(slot + other)
        return started

    for copy in weights:
        copy.wait()

    def d_arrive(i):
        src = lax.rem(e + i, NE)
        remote(disp.at[src], gath.at[t, src], d_send.at[i], d_recv.at[src], src, t).wait_recv()

    each(1, NE, d_arrive)

    accg[...] = jnp.zeros_like(accg)

    def gate_up(slot):
        part = wgu[pl.ds(pl.multiple_of(slot * WIDE, WIDE), WIDE), :]
        accg[...] += dot(gath[slot].reshape(SLOTS, WIDE), part, NN)

    spans = {1: (1, 3), 2: (3, 5), 3: (5, 7), 4: (7, 8)}
    started = ring(gath, g_send, g_recv, NE // 2, gate_up, lambda s: units(*spans[s]))
    gate = accg[:, 0:128]
    hb[t] = (gate / (1.0 + jnp.exp(-gate)) * accg[:, 128:256]).astype(BF16)

    accd[...] = jnp.zeros_like(accd)

    def down(slot):
        part = wd[pl.ds(pl.multiple_of(slot * 128, 128), 128), :]
        accd[...] += dot(hb[slot], part, NN)

    started += ring(hb, h_send, h_recv, SLOTS // 2, down, lambda s: None)
    res[...] = accd[...].astype(BF16).reshape(NE, CAP, WIDE)
    ret[e] = res[e]

    def b_copy(i):
        peer = lax.rem(e + i, NE)
        return remote(res.at[peer], ret.at[e], b_send.at[i], b_recv.at[e], peer, t)

    each(1, NE, lambda i: b_copy(i).start())

    def merge(i):
        zz = z - 1 - i
        remote(po_out.at[zz], po_in.at[zz], po_send.at[zz], po_recv.at[zz], e, t).wait_recv()
        remote(ps_out.at[zz], ps_in.at[zz], ps_send.at[zz], ps_recv.at[zz], e, t).wait_recv()
        top, new = top_s[...], ps_in[zz]
        newest = jnp.maximum(top, new)
        keep, add = jnp.exp2(top - newest), jnp.exp2(new - newest)
        top_s[...] = newest
        den_s[...] = den_s[...] * keep + add
        num_s[...] = num_s[...] * keep + po_in[zz].astype(F32) * add

    each(0, z, merge)
    ab[t] = (num_s[...] / den_s[...]).astype(BF16)
    accm[...] = jnp.zeros_like(accm)

    def project(slot):
        part = wo[pl.ds(pl.multiple_of(slot * HD, HD), HD), :]
        accm[...] += dot(ab[slot], part, TN)

    started += ring(ab, a_send, a_recv, HD // 2, project, lambda s: None)
    mix_ref[...] = accm[...].astype(BF16)

    def b_arrive(i):
        src = lax.rem(e + i, NE)
        remote(res.at[src], ret.at[src], b_send.at[i], b_recv.at[src], src, t).wait_recv()

    each(1, NE, b_arrive)
    back = ret[...].reshape(SLOTS, WIDE)
    square = lax.broadcasted_iota(jnp.int32, (TOK, TOK), 0) == lax.broadcasted_iota(
        jnp.int32, (TOK, TOK), 1
    )
    total = jnp.zeros((TOK, WIDE), F32)
    for i in range(2):
        scale = jnp.sum(
            jnp.where(square, rw_ref[i : i + 1, :], 0.0), axis=1, keepdims=True
        )
        total = total + dot(picks(i).astype(BF16), back, TN) * scale
    exp_ref[...] = total.astype(BF16)

    for copy in started:
        copy.wait_send()
    each(1, NTP, lambda i: tok_copy(i, lax.rem(t + i, NTP)).wait_send())
    for i in range(1, NX):
        for copy in kv_copies(i):
            copy.wait_send()
    each(1, NE, lambda i: d_copy(i).wait_send())
    each(0, z, lambda i: q_copy(i).wait_send())
    each(1, NE, lambda i: b_copy(i).wait_send())

    def po_sent(k):
        for copy in po_copies(k):
            copy.wait_send()

    each(z + 1, NZ, po_sent)


def body(
    queries, key_rows, values, forget_log, out_weight, expert_input, norm_gain,
    route_ids, route_weights, gate_weight, up_weight, down_weight,
):
    vmem = pl.BlockSpec(memory_space=pltpu.VMEM)
    hbm = pl.BlockSpec(memory_space=pl.ANY)
    dma = pltpu.SemaphoreType.DMA
    return pl.pallas_call(
        kernel,
        out_shape=(
            jax.ShapeDtypeStruct((ROWS, WIDE), BF16),
            jax.ShapeDtypeStruct((TOK, WIDE), BF16),
        ),
        in_specs=[vmem] * 8 + [hbm] * 4,
        out_specs=(vmem, vmem),
        scratch_shapes=[
            pltpu.VMEM((NX, ROWS, HD), BF16),
            pltpu.VMEM((NX, HD, ROWS), BF16),
            pltpu.VMEM((NZ, ROWS, HD), BF16),
            pltpu.VMEM((GROUP, 128), F32),
            pltpu.VMEM((NZ, HD, ROWS), BF16),
            pltpu.VMEM((NZ, 1, ROWS), F32),
            pltpu.VMEM((NZ, HD, ROWS), BF16),
            pltpu.VMEM((NZ, 1, ROWS), F32),
            pltpu.VMEM((1, WIDE), F32),
            pltpu.VMEM((1, WIDE), F32),
            pltpu.VMEM((HD, WIDE), F32),
            pltpu.VMEM((HD, ROWS), F32),
            pltpu.VMEM((1, ROWS), F32),
            pltpu.VMEM((1, ROWS), F32),
            pltpu.VMEM((NTP, 8, WIDE), F32),
            pltpu.VMEM((NTP, 8, WIDE), F32),
            pltpu.VMEM((NE, CAP, WIDE), BF16),
            pltpu.VMEM((NTP, NE, CAP, WIDE), BF16),
            pltpu.VMEM((SLOTS, WIDE), F32),
            pltpu.VMEM((NTP, SLOTS, 128), BF16),
            pltpu.VMEM((SLOTS, WIDE), F32),
            pltpu.VMEM((NE, CAP, WIDE), BF16),
            pltpu.VMEM((NE, CAP, WIDE), BF16),
            pltpu.VMEM((NTP, HD, ROWS), BF16),
            pltpu.VMEM((ROWS, WIDE), F32),
            pltpu.VMEM((D, 256), BF16),
            pltpu.VMEM((2048, WIDE), BF16),
            pltpu.VMEM((2048, WIDE), BF16),
            dma((4,)),
            dma((2 * NX,)), dma((2 * NX,)),
            dma((NZ,)), dma((NZ,)),
            dma((NTP,)), dma((NTP,)),
            dma((NE,)), dma((NE,)),
            dma((NZ,)), dma((NZ,)), dma((NZ,)), dma((NZ,)),
            dma((16,)), dma((NTP + 2,)),
            dma((16,)), dma((NTP + 2,)),
            dma((16,)), dma((NTP + 2,)),
            dma((NE,)), dma((NE,)),
        ],
        compiler_params=pltpu.CompilerParams(
            collective_id=0, has_side_effects=True, vmem_limit_bytes=56 * 1024 * 1024
        ),
    )(
        queries, key_rows, values, forget_log.reshape(1, -1), expert_input,
        norm_gain.reshape(1, -1), route_ids.T, route_weights.T,
        gate_weight.reshape(D, 128), up_weight.reshape(D, 128),
        down_weight.reshape(2048, WIDE), out_weight,
    )


def solution(mesh):
    placed = (
        P("ep", "tp"), P("ep", "tp"), P("ep", "tp"), P(None, "tp"), P(None, "tp"),
        P(("ep", "tp"), None), P(), P("ep", None), P("ep", None),
        P("ep", None, "tp"), P("ep", None, "tp"), P("ep", None, "tp"),
    )
    return jax.shard_map(
        body, mesh=mesh, in_specs=placed, out_specs=(P("ep", "tp"), P("ep", "tp")),
        check_vma=False,
    )
```

time: 521 us -> 124 us (0.24)
  the two profiles are of different devices: /device:TPU:1 before, /device:TPU:77 now
where the time goes in v1:
time: 124 us
  Pallas kernels  121 us (98%)
  local copies, waits for them, and re-layouts  2.33 us (2%)
    pallas_call x1, Pallas kernels, body(): pl.pallas_call(kernel, out_shape=(jax.ShapeDtypeStruct((ROWS, WIDE), BF16...  121 us

profile of v1, /device:TPU:77, one launch (start us, length us, event | category | flops | bytes accessed | tf_op | source)
XLA Modules:
  0.0 123.6 jit_solution(4617194959004574773)
XLA Ops:
  0.6 120.7 %shard_map.131 = (bf16[512,256]{1,0:T(8,128)(2,1)}, bf16[128,256]{1,0:T(8,128)(2,1)}) custom-call(bf16[512,128]{1,0:T(8,128)(2,1)} %q_ref.1, bf16[512,128]{1,0:T(8,128)(2,1)} %k_ref.1, bf16[512,128]{1,0:T(8,128)(2,1)} %v_ref.1, f32[1,16384]{1,0:T(1,128)} %bitcast.10, bf16[8,4096]{1,0:T(8,128)(2,1)} %xin_ref.1, f32[1,4096]{1,0:T(1,128)} %bitcast.11, ...), custom_call_target="tpu_custom_call" | custom-call | tf_op jit(solution)/shard_map/pallas_call | solution.py:382
  121.3 0.0 copy-start
  121.3 1.7 %copy.16 = bf16[512,256]{1,0:T(8,128)(2,1)} copy(bf16[512,256]{1,0:T(8,128)(2,1)} %get-tuple-element.4) | data formatting | bytes 524288
  123.0 0.0 copy-done
  123.0 0.6 copy.17
Async XLA Ops:
  121.3 1.7 %copy-start = (bf16[128,256]{1,0:T(8,128)(2,1)S(1)}, bf16[128,256]{1,0:T(8,128)(2,1)}, u32[]{:S(2)}) copy-start(bf16[128,256]{1,0:T(8,128)(2,1)} %get-tuple-element.5) | copy-start | bytes 196612
